TPU v7x, 32 devices: a whole 2x2x4 slice. The times are simulated.
32 devices in a mesh: sp: 8 (over z, x), dp: 4 (over y, core).
Axes of the slice: x: 2, y: 2, z: 4, core: 2. Of those that a mesh axis runs over, the one named last changes fastest.
Arguments:
- query_rows: bfloat16 [4, 1024, 2048], P('dp', 'sp'), may hold values from -6 to 6
- key_rows: bfloat16 [4, 1024, 2048], P('dp', 'sp'), may hold values from -6 to 6
- value_rows: bfloat16 [4, 1024, 2048], P('dp', 'sp'), may hold values from -6 to 6
- decay_low: bfloat16 [4, 1024, 128], P('dp', 'sp'), may hold values from -5 to 5
- rate_low: bfloat16 [4, 1024, 128], P('dp', 'sp'), may hold values from -4 to 4
- decay_up: bfloat16 [128, 2048], replicated, may hold values from -0.5 to 0.5
- rate_up: bfloat16 [128, 2048], replicated, may hold values from -0.5 to 0.5
- decay_base: float32 [2048], replicated, may hold values from -12 to -2
- norm_gain: float32 [2048], replicated, may hold values from 0.1 to 1.9
- out_weight: bfloat16 [2048, 2048], P(None, 'dp'), may hold values from -0.125 to 0.125
Outputs:
- layer_out: bfloat16 [4, 1024, 2048], P('dp', 'sp')
All inputs are finite; a program needn't handle non-finite values.
Results may differ from a plain program's by a relative error of at most 0.005.
Values may be sent and summed in bfloat16 or wider, within the bound.
A program may use at most 128 MiB of HBM per device.

v0:
```python
import functools
import math

import jax
import jax.numpy as jnp
from jax import lax
from jax.experimental import pallas as pl
from jax.experimental.pallas import tpu as pltpu
from jax.sharding import PartitionSpec as P

HEAD = 64
PAIR = 2 * HEAD

F32 = jnp.float32
BF16 = jnp.bfloat16


def mm(left, right):
    return lax.dot_general(left, right, (((1,), (0,)), ((), ())), preferred_element_type=F32)


def mm_nt(left, right):
    return lax.dot_general(left, right, (((1,), (1,)), ((), ())), preferred_element_type=F32)


def mm_tn(left, right):
    return lax.dot_general(left, right, (((0,), (0,)), ((), ())), preferred_element_type=F32)


def split(x):
    high = x.astype(BF16)
    return high, (x - high.astype(F32)).astype(BF16)


def mm3(left, right, form=mm):
    return form(left[0], right[0]) + form(left[0], right[1]) + form(left[1], right[0])


def iota(shape, dim):
    return lax.broadcasted_iota(jnp.int32, shape, dim)


def first_half(shape):
    return iota(shape, len(shape) - 1) < HEAD


def stack_pair(x):
    here = lax.rem(iota(x.shape, 1), PAIR) < HEAD
    zero = jnp.zeros_like(x)
    return jnp.concatenate([jnp.where(here, x, zero), jnp.where(here, zero, x)], axis=0)


def head_ones(scale):
    row = iota((2 * PAIR, PAIR), 0)
    col = iota((2 * PAIR, PAIR), 1)
    same = (lax.rem(row, PAIR) // HEAD) == (col // HEAD)
    return jnp.where(same, F32(scale), F32(0.0)).astype(BF16)


def head_sum(x, ones):
    return mm(jnp.concatenate(split(x), axis=1), ones)


def inverse_levels(strict_parts, size):
    row = iota((size, size), 0)
    col = iota((size, size), 1)
    eye = jnp.where(row == col, F32(1.0), F32(0.0))
    found = None
    block = 1
    while block < size:
        pick = (row // (2 * block) == col // (2 * block)) & (row // block != col // block) & (row > col)
        pieces = [jnp.where(pick, high, jnp.zeros_like(high)) for high, _ in strict_parts]
        if found is None:
            found = [eye.astype(BF16) - p for p in pieces]
        else:
            right = [mm(p, x).astype(BF16) for p, x in zip(pieces, found)]
            found = [x - mm(x, y).astype(BF16) for x, y in zip(found, right)]
        block *= 2
    out = []
    for (high, low), x in zip(strict_parts, found):
        product = mm(jnp.concatenate([high, low], axis=1), jnp.concatenate([x, x], axis=0))
        residual = ((eye - x.astype(F32)) - product).astype(BF16)
        out.append((x, mm(x, residual).astype(BF16)))
    return out


def gates(squashed, rate_low, decay_up, rate_up, base):
    decay_pre = (base + mm(squashed, decay_up)).astype(BF16).astype(F32)
    rate_pre = mm(rate_low, rate_up).astype(BF16).astype(F32)
    log_decay = -math.exp(-0.5) / (1.0 + jnp.exp(-decay_pre))
    rate = 1.0 / (1.0 + jnp.exp(-rate_pre))
    return log_decay, rate


def state_pairs(pairs):
    size = pairs[0][0].shape[0]
    middle = size // 2
    row = iota((size, size), 0)
    col = iota((size, size), 1)
    strict = row > col
    upto = jnp.where(row >= col, F32(1.0), F32(0.0)).astype(BF16)
    upto = jnp.concatenate([upto, upto], axis=1)
    ones = head_ones(1.0)
    made = []
    strict_parts = []
    for k, v, log_decay, rate in pairs:
        k = k.astype(F32)
        running = mm(upto, jnp.concatenate(split(log_decay), axis=0))
        centre = running[middle : middle + 1]
        final = running[size - 1 :]
        ahead_before = jnp.exp(running - log_decay - centre)
        behind = jnp.exp(centre - running)
        unit = k * lax.rsqrt(1.0 + head_sum(k * k, ones))
        at_end = jnp.exp(final - centre)
        erase_from = unit * ahead_before
        key_to = k * behind
        erase_to = unit * rate * behind
        left = split(stack_pair(erase_from))
        key_parts, erase_parts = split(key_to), split(erase_to)
        right = [jnp.concatenate(both, axis=0) for both in zip(key_parts, erase_parts)]
        grid = pair_grid(left, right)
        part = lambda i, j: jnp.where(
            strict, grid[i * size : (i + 1) * size, j * size : (j + 1) * size], 0.0
        )
        key_pairs = split(jnp.concatenate([part(0, 0), part(1, 0)], axis=1))
        strict_parts += [split(part(0, 1)), split(part(1, 1))]
        values = stack_pair(v)
        carried = mm(key_pairs[0], values) + mm(key_pairs[1], values)
        sides = jnp.concatenate([erase_from * jnp.exp(centre), carried], axis=1)
        made.append((
            v, sides, key_to * at_end, erase_to * at_end, jnp.exp(final),
            running, key_parts + erase_parts,
        ))
    inverses = inverse_levels(strict_parts, size)
    out = []
    for i, (v, sides, key_end, erase_end, decay_all, running, kept) in enumerate(made):
        xa, xb = inverses[2 * i], inverses[2 * i + 1]
        inv = tuple(jnp.concatenate([a, b], axis=1) for a, b in zip(xa, xb))
        solved = split(mm3(inv, split(stack_pair(sides))))
        key_parts = split(key_end)
        moved = mm3(split(erase_end), solved, mm_tn)
        gained = mm_tn(key_parts[0], v) + mm_tn(key_parts[1], v)
        row2 = iota((PAIR, PAIR), 0)
        col2 = iota((PAIR, PAIR), 1)
        transfer = jnp.where(row2 == col2, jnp.broadcast_to(decay_all, (PAIR, PAIR)), 0.0) - moved[:, :PAIR]
        added = gained - moved[:, PAIR:]
        half = first_half((HEAD, PAIR))
        fold = lambda x: jnp.where(half, x[:HEAD], x[HEAD:])
        halves = tuple(x[:, j : j + PAIR] for j in (0, PAIR) for x in solved)
        out.append((fold(transfer), fold(added), running) + kept + halves)
    return out


def pair_grid(left, right):
    return mm_nt(
        jnp.concatenate(left, axis=1), jnp.concatenate([right[0], right[0]], axis=1)
    ) + mm_nt(left[0], right[1])


def read_pair(q, v, running, kept, start, mean_ones):
    size = q.shape[0]
    within = iota((size, size), 0) >= iota((size, size), 1)
    centre = running[size // 2 : size // 2 + 1]
    read_mid = q.astype(F32) * jnp.exp(running - centre)
    left = split(stack_pair(read_mid))
    right = [jnp.concatenate([kept[i], kept[i + 2]], axis=0) for i in (0, 1)]
    solved = [jnp.concatenate([kept[i + 4], kept[i + 6]], axis=1) for i in (0, 1)]
    grid = pair_grid(left, right)
    part = lambda i, j: jnp.where(
        within, grid[i * size : (i + 1) * size, j * size : (j + 1) * size], 0.0
    )
    read_keys = split(jnp.concatenate([part(0, 0), part(1, 0)], axis=1))
    read_erase = split(jnp.concatenate([part(0, 1), part(1, 1)], axis=1))
    values = stack_pair(v)
    here = mm(read_keys[0], values) + mm(read_keys[1], values)
    taken = mm3(read_erase, [stack_pair(x) for x in solved])
    read_state = read_mid * jnp.exp(centre) - taken[:, :PAIR]
    readout = mm3(split(read_state), split(stack_pair(start))) + here - taken[:, PAIR:]
    centred = readout - head_sum(readout, mean_ones)
    variance = head_sum(centred * centred, mean_ones)
    return centred * lax.rsqrt(variance + 1.0)


def fused_kernel(devices, columns, lanes, pieces, q_ref, k_ref, v_ref, low_ref, rate_ref, dup_ref,
                 rup_ref, base_ref, gain_ref, weight_ref, out_ref, weights, transfer_ref, added_ref,
                 running_ref, kept_ref, mix_ref, start_buf, end_buf, own_sem, near_sem, far_send,
                 far_recv, pass_send, pass_recv, send_sem, recv_sem):
    me = lax.axis_index("sp")
    mine = lax.axis_index("dp")
    partner = mine + 1 - 2 * lax.rem(mine, 2)
    width = q_ref.shape[1]
    groups = width // lanes
    count = lanes // PAIR
    others = columns // 2 - 1
    cols = weight_ref.shape[1]
    piece = weight_ref.shape[0] // pieces
    has_left = me > 0
    has_right = me < devices - 1
    barrier = pltpu.get_barrier_semaphore()

    def greet(where):
        pl.semaphore_signal(barrier, inc=1, device_id=where, device_id_type=pl.DeviceIdType.MESH)

    def ahead_of(j):
        return lax.rem(mine + 2 * (j + 1), columns)

    def behind_of(j):
        return lax.rem(mine + columns - 2 * (j + 1), columns)

    def remote(src, dst, send, recv, where):
        return pltpu.make_async_remote_copy(
            src_ref=src, dst_ref=dst, send_sem=send, recv_sem=recv,
            device_id=where, device_id_type=pl.DeviceIdType.MESH,
        )

    greet({"dp": partner})
    for j in range(others):
        greet({"dp": ahead_of(j)})

    @pl.when(has_left)
    def _():
        greet({"sp": me - 1})

    @pl.when(has_right)
    def _():
        greet({"sp": me + 1})

    own = pltpu.make_async_copy(weight_ref, weights.at[mine], own_sem)
    own.start()
    pl.semaphore_wait(
        barrier, 1 + others + jnp.minimum(me, 1) + jnp.minimum(devices - 1 - me, 1)
    )

    def rows(c):
        return pl.ds(c * piece, piece)

    def far(j, c):
        return remote(
            weight_ref.at[rows(c)], weights.at[mine, rows(c)],
            far_send.at[j, c], far_recv.at[j, c], {"dp": ahead_of(j)},
        )

    def passed(j, c):
        return remote(
            weights.at[behind_of(j), rows(c)], weights.at[behind_of(j), rows(c)],
            pass_send.at[j, c], pass_recv.at[j, c], {"dp": partner},
        )

    near = remote(weight_ref, weights.at[mine], near_sem.at[0], near_sem.at[1], {"dp": partner})
    for j in range(others):
        for c in range(pieces):
            far(j, c).start()
    near.start()

    def forward(c):
        for j in range(others):
            far(j, c).wait_recv()
            passed(j, c).start()

    def lanes_of(g):
        return pl.ds(pl.multiple_of(g * lanes, lanes), lanes)

    def cut(x, i):
        return x[:, i * PAIR : (i + 1) * PAIR]

    def make(g):
        at = lanes_of(g)
        squashed = jnp.tanh(low_ref[...].astype(F32)).astype(BF16)
        log_decay, rate = gates(
            squashed, rate_ref[...], dup_ref[:, at], rup_ref[:, at], base_ref[:, at]
        )
        k, v = k_ref[:, at], v_ref[:, at]
        pairs = [tuple(cut(x, i) for x in (k, v, log_decay, rate)) for i in range(count)]
        parts = [jnp.concatenate(part, axis=1) for part in zip(*state_pairs(pairs))]
        transfer_ref[:, at], added_ref[:, at], running_ref[:, at] = parts[:3]
        for i, part in enumerate(parts[3:]):
            kept_ref[i, :, at] = part

    def copy(g):
        return remote(
            end_buf.at[g], start_buf.at[g], send_sem.at[g], recv_sem.at[g],
            {"sp": lax.rem(me + 1, devices)},
        )

    def advance(g):
        @pl.when(has_left)
        def _():
            copy(g).wait_recv()

        at = lanes_of(g)
        transfer, added, start = transfer_ref[:, at], added_ref[:, at], start_buf[g]
        ends = [
            mm3(split(cut(transfer, i)), split(stack_pair(cut(start, i)))) for i in range(count)
        ]
        end_buf[g] = jnp.concatenate(ends, axis=1) + added

        @pl.when(has_right)
        def _():
            copy(g).start()

    mean_ones = head_ones(1.0 / HEAD)

    def read(g):
        at = lanes_of(g)
        q, v, running, gain, start = (
            q_ref[:, at], v_ref[:, at], running_ref[:, at], gain_ref[:, at], start_buf[g]
        )
        kept = [kept_ref[j, :, at] for j in range(kept_ref.shape[0])]
        normed = [
            read_pair(
                cut(q, i), cut(v, i), cut(running, i), [cut(x, i) for x in kept],
                cut(start, i), mean_ones,
            )
            for i in range(count)
        ]
        mix_ref[:, at] = (jnp.concatenate(normed, axis=1) * gain).astype(BF16)

    @pl.when(jnp.logical_not(has_left))
    def _():
        start_buf[...] = jnp.zeros_like(start_buf)

    slots = max(groups, devices) + groups
    early = min(pieces, (slots - 1) // 4)

    def slot(s, carry):
        @pl.when(s < groups)
        def _():
            make(s)

        @pl.when((s >= me) & (s < me + groups))
        def _():
            advance(s - me)

        first = jnp.maximum(groups, me + 1)

        @pl.when((s >= first) & (s < first + groups))
        def _():
            read(s - first)

        c = s // 4 - 1

        @pl.when((lax.rem(s, 4) == 0) & (c >= 0) & (c < early))
        def _():
            forward(c)

        return carry

    lax.fori_loop(0, slots, slot, 0)
    for c in range(early, pieces):
        forward(c)

    def project(d):
        at = pl.ds(pl.multiple_of(d * cols, cols), cols)
        out_ref[:, at] = mm(mix_ref[...], weights[d]).astype(BF16)

    own.wait()
    project(mine)
    near.wait_recv()
    project(partner)
    for j in range(others):
        project(behind_of(j))
    for j in range(others):
        for c in range(pieces):
            passed(j, c).wait_recv()
        project(lax.rem(partner + columns - 2 * (j + 1), columns))

    near.wait_send()
    for j in range(others):
        for c in range(pieces):
            far(j, c).wait_send()
            passed(j, c).wait_send()

    @pl.when(has_right)
    def _():
        for g in range(groups):
            copy(g).wait_send()


def per_device(devices, columns, query_rows, key_rows, value_rows, decay_low, rate_low, decay_up,
               rate_up, decay_base, norm_gain, out_weight):
    q = query_rows[0]
    size, width = q.shape
    depth, cols = out_weight.shape
    lanes = PAIR * math.gcd(width // PAIR, 2)
    groups = width // lanes
    pieces = 4
    others = columns // 2 - 1
    vmem = pl.BlockSpec(memory_space=pltpu.VMEM)
    dma = lambda *dims: pltpu.SemaphoreType.DMA(dims)
    out = pl.pallas_call(
        functools.partial(fused_kernel, devices, columns, lanes, pieces),
        in_specs=[vmem] * 9 + [pl.BlockSpec(memory_space=pl.ANY)],
        out_specs=vmem,
        out_shape=jax.ShapeDtypeStruct((size, columns * cols), BF16),
        scratch_shapes=[
            pltpu.VMEM((columns, depth, cols), BF16),
            pltpu.VMEM((HEAD, width), F32),
            pltpu.VMEM((HEAD, width), F32),
            pltpu.VMEM((size, width), F32),
            pltpu.VMEM((8, size, width), BF16),
            pltpu.VMEM((size, width), BF16),
            pltpu.VMEM((groups, HEAD, lanes), F32),
            pltpu.VMEM((groups, HEAD, lanes), F32),
            pltpu.SemaphoreType.DMA,
            dma(2),
            dma(others, pieces),
            dma(others, pieces),
            dma(others, pieces),
            dma(others, pieces),
            dma(groups),
            dma(groups),
        ],
        compiler_params=pltpu.CompilerParams(collective_id=0, has_side_effects=True),
        name="fused_mixer",
    )(
        q, key_rows[0], value_rows[0], decay_low[0], rate_low[0], decay_up, rate_up,
        decay_base[None], norm_gain[None], out_weight,
    )
    return out[None]


def solution(mesh):
    in_specs = (
        P("dp", "sp", None),
        P("dp", "sp", None),
        P("dp", "sp", None),
        P("dp", "sp", None),
        P("dp", "sp", None),
        P(),
        P(),
        P(),
        P(),
        P(None, "dp"),
    )
    return jax.shard_map(
        functools.partial(per_device, mesh.shape["sp"], mesh.shape["dp"]),
        mesh=mesh, in_specs=in_specs, out_specs=P("dp", "sp", None), check_vma=False,
    )
```

profile of v0, /device:TPU:27, one launch (start us, length us, event | category | flops | bytes accessed | tf_op | source)
XLA Modules:
  0.0 69.1 jit_solution(4223556825301929474)
XLA Ops:
  0.0 67.2 %fused_mixer.1 = bf16[128,2048]{1,0:T(8,128)(2,1)} custom-call(bf16[128,2048]{1,0:T(8,128)(2,1)} %bitcast.9, bf16[128,2048]{1,0:T(8,128)(2,1)} %bitcast.10, bf16[128,2048]{1,0:T(8,128)(2,1)} %bitcast.11, bf16[128,128]{1,0:T(8,128)(2,1)} %bitcast.12, bf16[128,128]{1,0:T(8,128)(2,1)} %bitcast.13, bf16[128,2048]{1,0:T(8,128)(2,1)} %dup_ref.1, ...), custom_call_target="tpu_custom_call" | custom-call | tf_op jit(solution)/shard_map/fused_mixer/pallas_call | solution.py:390
  67.2 1.9 %copy.12 = bf16[1,128,2048]{2,1,0:T(8,128)(2,1)} copy(bf16[1,128,2048]{2,1,0:T(8,128)(2,1)} %bitcast.8) | data formatting | bytes 1048576
where the time goes:
time: 69.3 us; the launch traced here: 69.1 us
  Pallas kernels  67.2 us (97%)
  local copies, waits for them, and re-layouts  1.88 us (3%)
    pallas_call x1, Pallas kernels, per_device(): pl.pallas_call(functools.partial(fused_kernel, devices, columns, lanes, p...  67.2 us
    unnamed x1, local copies, waits for them, and re-layouts  1.88 us

commit v1 on v0

v1 whole, which is shorter than its diff:
```python
import functools
import math

import jax
import jax.numpy as jnp
from jax import lax
from jax.experimental import pallas as pl
from jax.experimental.pallas import tpu as pltpu
from jax.sharding import PartitionSpec as P

HEAD = 64
PAIR = 2 * HEAD
WIDE = 4

F32 = jnp.float32
BF16 = jnp.bfloat16


def mm(left, right):
    return lax.dot_general(left, right, (((1,), (0,)), ((), ())), preferred_element_type=F32)


def mm_nt(left, right):
    return lax.dot_general(left, right, (((1,), (1,)), ((), ())), preferred_element_type=F32)


def mm_tn(left, right):
    return lax.dot_general(left, right, (((0,), (0,)), ((), ())), preferred_element_type=F32)


def split(x):
    high = x.astype(BF16)
    return high, (x - high.astype(F32)).astype(BF16)


def mm_ab(left, right, form=mm):
    return form(left[0], right[0]) + form(left[0], right[1]) + form(left[1], right[0])


def beside(*parts):
    return jnp.concatenate(parts, axis=1)


def below(*parts):
    return jnp.concatenate(parts, axis=0)


def swap(x):
    return pltpu.roll(x, HEAD, 1)


def iota(shape, dim):
    return lax.broadcasted_iota(jnp.int32, shape, dim)


def first_half(shape):
    return iota(shape, len(shape) - 1) < HEAD


def stack_pair(x):
    here = lax.rem(iota(x.shape, 1), PAIR) < HEAD
    zero = jnp.zeros_like(x)
    return jnp.concatenate([jnp.where(here, x, zero), jnp.where(here, zero, x)], axis=0)


def head_ones(scale):
    row = iota((PAIR, PAIR), 0)
    col = iota((PAIR, PAIR), 1)
    return jnp.where(row // HEAD == col // HEAD, F32(scale), F32(0.0)).astype(BF16)


def head_sum(x, ones):
    return mm(beside(*split(x)), below(ones, ones))


def solve(parts, size):
    row = iota((size, size), 0)
    col = iota((size, size), 1)
    whole = [beside(z, y) for z, y in parts]
    block = 1
    while block < size:
        last = 2 * block == size
        pick = (row // (2 * block) == col // (2 * block)) & (row // block != col // block)
        fine = block % 16 != 0
        spans = [(0, size)] if fine else [(r + block, r + 2 * block) for r in range(0, size, 2 * block)]
        found = []
        for x in whole:
            high, low = split(x)
            move = jnp.where(pick, high[:, :size], jnp.zeros_like(high[:, :size]))
            move = move if fine else below(*[move[a:b] for a, b in spans])
            if last:
                x, high, low = x[:, size:], high[:, size:], low[:, size:]
            step = mm(beside(move, move), below(high, low))
            if fine:
                found.append(x - step)
            else:
                rows = []
                for i, (a, b) in enumerate(spans):
                    rows += [x[a - block : a], x[a:b] - step[i * block : (i + 1) * block]]
                found.append(below(*rows))
        whole = found
        block *= 2
    return whole


def gates(squashed, rate_low, decay_up, rate_up, base):
    decay_pre = (base + mm(squashed, decay_up)).astype(BF16).astype(F32)
    rate_pre = mm(rate_low, rate_up).astype(BF16).astype(F32)
    log_decay = -math.exp(-0.5) / (1.0 + jnp.exp(-decay_pre))
    rate = 1.0 / (1.0 + jnp.exp(-rate_pre))
    return log_decay, rate


def pair_grid(left, right):
    return mm_nt(beside(*left), beside(right[0], right[0])) + mm_nt(left[0], right[1])


def make_pairs(pairs):
    size = pairs[0][0].shape[0]
    middle = size // 2
    row = iota((size, size), 0)
    col = iota((size, size), 1)
    strict = row > col
    within = row >= col
    upto = jnp.where(within, F32(1.0), F32(0.0)).astype(BF16)
    upto = beside(upto, upto)
    ones = head_ones(1.0)
    half = first_half((size, PAIR))
    runs = [mm(upto, below(*split(p[3]))) for p in pairs]
    sums = []
    for p in pairs:
        k = p[1].astype(F32)
        sums.append(mm((k * k).astype(BF16), ones))
    made = []
    for (q, k, v, log_decay, rate), running, total in zip(pairs, runs, sums):
        k = k.astype(F32)
        centre = running[middle : middle + 1]
        final = running[size - 1 :]
        behind = jnp.exp(centre - running)
        unit = k * lax.rsqrt(1.0 + total)
        erase_from = unit * jnp.exp(running - log_decay - centre)
        read_from = q.astype(F32) * jnp.exp(running - centre)
        key_to = k * behind
        erase_to = unit * rate * behind
        made.append((erase_from, read_from, key_to, erase_to, centre, final))
    grids = []
    for erase_from, read_from, key_to, erase_to, _, _ in made:
        left = split(below(stack_pair(erase_from), stack_pair(read_from)))
        grids.append(pair_grid(left, split(below(key_to, erase_to))))

    def part(grid, i, j, keep):
        return jnp.where(keep, grid[i * size : (i + 1) * size, j * size : (j + 1) * size], 0.0)

    stacked = [stack_pair(p[2]) for p in pairs]
    parts = []
    for grid, values, (erase_from, _, _, _, centre, _) in zip(grids, stacked, made):
        keys = split(beside(part(grid, 0, 0, strict), part(grid, 1, 0, strict)))
        carried = mm(keys[0], values) + mm(keys[1], values)
        erase = erase_from * jnp.exp(centre)
        parts.append((part(grid, 0, 1, strict), jnp.where(half, erase, swap(carried))))
        parts.append((part(grid, 1, 1, strict), jnp.where(half, swap(erase), carried)))
    solved = solve(parts, size)
    row2 = iota((PAIR, PAIR), 0)
    col2 = iota((PAIR, PAIR), 1)
    half2 = first_half((HEAD, PAIR))
    fold = lambda x: jnp.where(half2, x[:HEAD], x[HEAD:])
    out = []
    for i, (p, grid, values, (_, read_from, key_to, erase_to, centre, final)) in enumerate(
        zip(pairs, grids, stacked, made)
    ):
        a, b = solved[2 * i], solved[2 * i + 1]
        both = split(beside(jnp.where(half, a, swap(b)), jnp.where(half, swap(a), b)))
        at_end = jnp.exp(final - centre)
        erase_end = split(erase_to * at_end)
        key_end = split(key_to * at_end)
        moved = mm_tn(below(*erase_end), below(both[0], both[0])) + mm_tn(erase_end[0], both[1])
        gained = mm_tn(below(*key_end), below(p[2], p[2]))
        read_keys = split(beside(part(grid, 2, 0, within), part(grid, 3, 0, within)))
        read_erase = split(beside(part(grid, 2, 1, within), part(grid, 3, 1, within)))
        here = mm(read_keys[0], values) + mm(read_keys[1], values)
        taken = mm_ab(read_erase, [stack_pair(x) for x in both])
        decay = jnp.broadcast_to(jnp.exp(final), (PAIR, PAIR))
        transfer = jnp.where(row2 == col2, decay, 0.0) - moved[:, :PAIR]
        added = gained - moved[:, PAIR:]
        read_state = read_from * jnp.exp(centre) - taken[:, :PAIR]
        out.append(
            split(below(fold(transfer), read_state))
            + (below(fold(added), here - taken[:, PAIR:]),)
        )
    return out


def normed(readout, ones):
    centred = readout - head_sum(readout, ones)
    variance = head_sum(centred * centred, ones)
    return centred * lax.rsqrt(variance + 1.0)


def fused_kernel(devices, columns, wide, lanes, pieces, q_ref, k_ref, v_ref, low_ref, rate_ref,
                 dup_ref, rup_ref, base_ref, gain_ref, weight_ref, out_ref, weights, maps_ref,
                 adds_ref, mix_ref, start_buf, end_buf, own_sem, near_sem, far_send, far_recv,
                 pass_send, pass_recv, send_sem, recv_sem):
    me = lax.axis_index("sp")
    mine = lax.axis_index("dp")
    partner = mine + 1 - 2 * lax.rem(mine, 2)
    width = q_ref.shape[1]
    groups = width // lanes
    blocks = width // wide
    each = wide // lanes
    others = columns // 2 - 1
    cols = weight_ref.shape[1]
    piece = weight_ref.shape[0] // pieces
    has_left = me > 0
    has_right = me < devices - 1
    barrier = pltpu.get_barrier_semaphore()

    def greet(where):
        pl.semaphore_signal(barrier, inc=1, device_id=where, device_id_type=pl.DeviceIdType.MESH)

    def ahead_of(j):
        return lax.rem(mine + 2 * (j + 1), columns)

    def behind_of(j):
        return lax.rem(mine + columns - 2 * (j + 1), columns)

    def remote(src, dst, send, recv, where):
        return pltpu.make_async_remote_copy(
            src_ref=src, dst_ref=dst, send_sem=send, recv_sem=recv,
            device_id=where, device_id_type=pl.DeviceIdType.MESH,
        )

    greet({"dp": partner})
    for j in range(others):
        greet({"dp": ahead_of(j)})

    @pl.when(has_left)
    def _():
        greet({"sp": me - 1})

    @pl.when(has_right)
    def _():
        greet({"sp": me + 1})

    own = pltpu.make_async_copy(weight_ref, weights.at[mine], own_sem)
    own.start()
    pl.semaphore_wait(
        barrier, 1 + others + jnp.minimum(me, 1) + jnp.minimum(devices - 1 - me, 1)
    )

    def rows(c):
        return pl.ds(c * piece, piece)

    def far(j, c):
        return remote(
            weight_ref.at[rows(c)], weights.at[mine, rows(c)],
            far_send.at[j, c], far_recv.at[j, c], {"dp": ahead_of(j)},
        )

    def passed(j, c):
        return remote(
            weights.at[behind_of(j), rows(c)], weights.at[behind_of(j), rows(c)],
            pass_send.at[j, c], pass_recv.at[j, c], {"dp": partner},
        )

    near = remote(weight_ref, weights.at[mine], near_sem.at[0], near_sem.at[1], {"dp": partner})
    for j in range(others):
        for c in range(pieces):
            far(j, c).start()
    near.start()

    def forward(c):
        for j in range(others):
            far(j, c).wait_recv()
            passed(j, c).start()

    def lanes_of(g, size):
        return pl.ds(pl.multiple_of(g * size, size), size)

    def cut(x, i):
        return x[:, i * PAIR : (i + 1) * PAIR]

    def make(b):
        at = lanes_of(b, wide)
        squashed = jnp.tanh(low_ref[...].astype(F32)).astype(BF16)
        log_decay, rate = gates(
            squashed, rate_ref[...], dup_ref[:, at], rup_ref[:, at], base_ref[:, at]
        )
        q, k, v = q_ref[:, at], k_ref[:, at], v_ref[:, at]
        made = make_pairs(
            [tuple(cut(x, i) for x in (q, k, v, log_decay, rate)) for i in range(wide // PAIR)]
        )
        high, low, adds = [beside(*part) for part in zip(*made)]
        maps_ref[0, :, at], maps_ref[1, :, at], adds_ref[:, at] = high, low, adds

    def copy(g):
        return remote(
            end_buf.at[g], start_buf.at[g], send_sem.at[g], recv_sem.at[g],
            {"sp": lax.rem(me + 1, devices)},
        )

    mean_ones = head_ones(1.0 / HEAD)

    def advance(g):
        at = lanes_of(g, lanes)

        @pl.when(has_left)
        def _():
            copy(g).wait_recv()

        start = start_buf[g]
        states = [stack_pair(cut(start, i)) for i in range(lanes // PAIR)]
        states = [below(x, x) for x in states]

        def apply(a, b):
            high, low, adds = maps_ref[0, a:b, at], maps_ref[1, a:b, at], adds_ref[a:b, at]
            return [
                mm(beside(cut(high, i), cut(low, i)), x) + cut(adds, i)
                for i, x in enumerate(states)
            ]

        end_buf[g] = beside(*apply(0, HEAD)).astype(BF16)

        @pl.when(has_right)
        def _():
            copy(g).start()

        readouts = apply(HEAD, maps_ref.shape[1])
        mix = beside(*[normed(x, mean_ones) for x in readouts])
        mix_ref[:, at] = (mix * gain_ref[:, at]).astype(BF16)

    @pl.when(jnp.logical_not(has_left))
    def _():
        start_buf[...] = jnp.zeros_like(start_buf)

    def slot(s, carry):
        @pl.when(s < blocks)
        def _():
            make(s)

        @pl.when((s >= me) & (s < me + blocks))
        def _():
            for i in range(each):
                advance((s - me) * each + i)

        return carry

    lax.fori_loop(0, blocks + devices - 1, slot, 0)
    for c in range(pieces):
        forward(c)

    def project(d):
        at = pl.ds(pl.multiple_of(d * cols, cols), cols)
        out_ref[:, at] = mm(mix_ref[...], weights[d]).astype(BF16)

    own.wait()
    project(mine)
    near.wait_recv()
    project(partner)
    for j in range(others):
        project(behind_of(j))
    for j in range(others):
        for c in range(pieces):
            passed(j, c).wait_recv()
        project(lax.rem(partner + columns - 2 * (j + 1), columns))

    near.wait_send()
    for j in range(others):
        for c in range(pieces):
            far(j, c).wait_send()
            passed(j, c).wait_send()

    @pl.when(has_right)
    def _():
        for g in range(groups):
            copy(g).wait_send()


def per_device(devices, columns, query_rows, key_rows, value_rows, decay_low, rate_low, decay_up,
               rate_up, decay_base, norm_gain, out_weight):
    q = query_rows[0]
    size, width = q.shape
    depth, cols = out_weight.shape
    wide = PAIR * math.gcd(width // PAIR, WIDE)
    lanes = PAIR * math.gcd(wide // PAIR, 2)
    groups = width // lanes
    pieces = 4
    others = columns // 2 - 1
    vmem = pl.BlockSpec(memory_space=pltpu.VMEM)
    dma = lambda *dims: pltpu.SemaphoreType.DMA(dims)
    out = pl.pallas_call(
        functools.partial(fused_kernel, devices, columns, wide, lanes, pieces),
        in_specs=[vmem] * 9 + [pl.BlockSpec(memory_space=pl.ANY)],
        out_specs=vmem,
        out_shape=jax.ShapeDtypeStruct((size, columns * cols), BF16),
        scratch_shapes=[
            pltpu.VMEM((columns, depth, cols), BF16),
            pltpu.VMEM((2, HEAD + size, width), BF16),
            pltpu.VMEM((HEAD + size, width), F32),
            pltpu.VMEM((size, width), BF16),
            pltpu.VMEM((groups, HEAD, lanes), BF16),
            pltpu.VMEM((groups, HEAD, lanes), BF16),
            pltpu.SemaphoreType.DMA,
            dma(2),
            dma(others, pieces),
            dma(others, pieces),
            dma(others, pieces),
            dma(others, pieces),
            dma(groups),
            dma(groups),
        ],
        compiler_params=pltpu.CompilerParams(collective_id=0, has_side_effects=True),
        name="fused_mixer",
    )(
        q, key_rows[0], value_rows[0], decay_low[0], rate_low[0], decay_up, rate_up,
        decay_base[None], norm_gain[None], out_weight,
    )
    return out[None]


def solution(mesh):
    in_specs = (
        P("dp", "sp", None),
        P("dp", "sp", None),
        P("dp", "sp", None),
        P("dp", "sp", None),
        P("dp", "sp", None),
        P(),
        P(),
        P(),
        P(),
        P(None, "dp"),
    )
    return jax.shard_map(
        functools.partial(per_device, mesh.shape["sp"], mesh.shape["dp"]),
        mesh=mesh, in_specs=in_specs, out_specs=P("dp", "sp", None), check_vma=False,
    )
```

time: 69.3 us -> 56.8 us (0.82)
  the two profiles are of different devices: /device:TPU:27 before, /device:TPU:1 now
where the time goes in v1:
time: 56.8 us; the launch traced here: 56.7 us
  Pallas kernels  54.8 us (96%)
  local copies, waits for them, and re-layouts  1.88 us (3%)
    pallas_call x1, Pallas kernels, per_device(): pl.pallas_call(functools.partial(fused_kernel, devices, columns, wide, la...  54.8 us
    unnamed x1, local copies, waits for them, and re-layouts  1.88 us

profile of v1, /device:TPU:1, one launch (start us, length us, event | category | flops | bytes accessed | tf_op | source)
XLA Modules:
  0.0 56.7 jit_solution(14121537034293788965)
XLA Ops:
  0.0 54.8 %fused_mixer.1 = bf16[128,2048]{1,0:T(8,128)(2,1)} custom-call(bf16[128,2048]{1,0:T(8,128)(2,1)} %bitcast.9, bf16[128,2048]{1,0:T(8,128)(2,1)} %bitcast.10, bf16[128,2048]{1,0:T(8,128)(2,1)} %bitcast.11, bf16[128,128]{1,0:T(8,128)(2,1)} %bitcast.12, bf16[128,128]{1,0:T(8,128)(2,1)} %bitcast.13, bf16[128,2048]{1,0:T(8,128)(2,1)} %dup_ref.1, ...), custom_call_target="tpu_custom_call" | custom-call | tf_op jit(solution)/shard_map/fused_mixer/pallas_call | solution.py:390
  54.8 1.9 %copy.12 = bf16[1,128,2048]{2,1,0:T(8,128)(2,1)} copy(bf16[1,128,2048]{2,1,0:T(8,128)(2,1)} %bitcast.8) | data formatting | bytes 1048576

commit v2 on v1

v2 whole, which is shorter than its diff:
```python
import functools
import math

import jax
import jax.numpy as jnp
from jax import lax
from jax.experimental import pallas as pl
from jax.experimental.pallas import tpu as pltpu
from jax.sharding import PartitionSpec as P

HEAD = 64
PAIR = 2 * HEAD
WIDE = 4

F32 = jnp.float32
BF16 = jnp.bfloat16


def mm(left, right):
    return lax.dot_general(left, right, (((1,), (0,)), ((), ())), preferred_element_type=F32)


def mm_nt(left, right):
    return lax.dot_general(left, right, (((1,), (1,)), ((), ())), preferred_element_type=F32)


def mm_tn(left, right):
    return lax.dot_general(left, right, (((0,), (0,)), ((), ())), preferred_element_type=F32)


def split(x):
    high = x.astype(BF16)
    return high, (x - high.astype(F32)).astype(BF16)


def mm_ab(left, right, form=mm):
    return form(left[0], right[0]) + form(left[0], right[1]) + form(left[1], right[0])


def beside(*parts):
    return jnp.concatenate(parts, axis=1)


def below(*parts):
    return jnp.concatenate(parts, axis=0)


def swap(x):
    return pltpu.roll(x, HEAD, 1)


def iota(shape, dim):
    return lax.broadcasted_iota(jnp.int32, shape, dim)


def first_half(shape):
    return iota(shape, len(shape) - 1) < HEAD


def stack_pair(x):
    here = lax.rem(iota(x.shape, 1), PAIR) < HEAD
    zero = jnp.zeros_like(x)
    return jnp.concatenate([jnp.where(here, x, zero), jnp.where(here, zero, x)], axis=0)


def head_ones(scale):
    row = iota((PAIR, PAIR), 0)
    col = iota((PAIR, PAIR), 1)
    return jnp.where(row // HEAD == col // HEAD, F32(scale), F32(0.0)).astype(BF16)


def head_sum(x, ones):
    return mm(beside(*split(x)), below(ones, ones))


def solve(parts, size):
    row = iota((size, size), 0)
    col = iota((size, size), 1)
    whole = [beside(z, y) for z, y in parts]
    block = 1
    while block < size:
        last = 2 * block == size
        pick = (row // (2 * block) == col // (2 * block)) & (row // block != col // block)
        fine = block % 16 != 0
        spans = [(0, size)] if fine else [(r + block, r + 2 * block) for r in range(0, size, 2 * block)]
        found = []
        for x in whole:
            high, low = split(x)
            move = jnp.where(pick, high[:, :size], jnp.zeros_like(high[:, :size]))
            move = move if fine else below(*[move[a:b] for a, b in spans])
            if last:
                x, high, low = x[:, size:], high[:, size:], low[:, size:]
            step = mm(beside(move, move), below(high, low))
            if fine:
                found.append(x - step)
            else:
                rows = []
                for i, (a, b) in enumerate(spans):
                    rows += [x[a - block : a], x[a:b] - step[i * block : (i + 1) * block]]
                found.append(below(*rows))
        whole = found
        block *= 2
    return whole


def gates(squashed, rate_low, decay_up, rate_up, base):
    decay_pre = (base + mm(squashed, decay_up)).astype(BF16).astype(F32)
    rate_pre = mm(rate_low, rate_up).astype(BF16).astype(F32)
    log_decay = -math.exp(-0.5) / (1.0 + jnp.exp(-decay_pre))
    rate = 1.0 / (1.0 + jnp.exp(-rate_pre))
    return log_decay, rate


def pair_grid(left, right):
    return mm_nt(beside(*left), beside(right[0], right[0])) + mm_nt(left[0], right[1])


def chunk_maps(pairs):
    size = pairs[0][0].shape[0]
    middle = size // 2
    row = iota((size, size), 0)
    col = iota((size, size), 1)
    strict = row > col
    upto = jnp.where(row >= col, F32(1.0), F32(0.0)).astype(BF16)
    upto = beside(upto, upto)
    ones = head_ones(1.0)
    half = first_half((size, PAIR))
    runs = [mm(upto, below(*split(p[2]))) for p in pairs]
    sums = []
    for p in pairs:
        k = p[0].astype(F32)
        sums.append(head_sum(k * k, ones))
    made = []
    for (k, v, log_decay, rate), running, total in zip(pairs, runs, sums):
        k = k.astype(F32)
        centre = running[middle : middle + 1]
        behind = jnp.exp(centre - running)
        unit = k * lax.rsqrt(1.0 + total)
        erase_from = unit * jnp.exp(running - log_decay - centre)
        made.append((erase_from, k * behind, unit * rate * behind, centre, running[size - 1 :]))
    grids = []
    keeps = []
    for erase_from, key_to, erase_to, _, _ in made:
        keeps.append(split(key_to) + split(erase_to))
        key_high, key_low, erase_high, erase_low = keeps[-1]
        right = below(key_high, erase_high), below(key_low, erase_low)
        grids.append(pair_grid(split(stack_pair(erase_from)), right))

    def part(grid, i, j):
        return jnp.where(
            strict, grid[i * size : (i + 1) * size, j * size : (j + 1) * size], 0.0
        )

    parts = []
    for p, grid, (erase_from, _, _, centre, _) in zip(pairs, grids, made):
        values = stack_pair(p[1])
        keys = split(beside(part(grid, 0, 0), part(grid, 1, 0)))
        carried = mm(keys[0], values) + mm(keys[1], values)
        erase = erase_from * jnp.exp(centre)
        parts.append((part(grid, 0, 1), jnp.where(half, erase, swap(carried))))
        parts.append((part(grid, 1, 1), jnp.where(half, swap(erase), carried)))
    solved = solve(parts, size)
    row2 = iota((PAIR, PAIR), 0)
    col2 = iota((PAIR, PAIR), 1)
    half2 = first_half((HEAD, PAIR))
    fold = lambda x: jnp.where(half2, x[:HEAD], x[HEAD:])
    out = []
    for i, (p, keep, running, (_, key_to, erase_to, centre, final)) in enumerate(
        zip(pairs, keeps, runs, made)
    ):
        a, b = solved[2 * i], solved[2 * i + 1]
        both = split(beside(jnp.where(half, a, swap(b)), jnp.where(half, swap(a), b)))
        at_end = jnp.exp(final - centre)
        erase_end = split(erase_to * at_end)
        key_end = split(key_to * at_end)
        moved = mm_tn(below(*erase_end), below(both[0], both[0])) + mm_tn(erase_end[0], both[1])
        gained = mm_tn(below(*key_end), below(p[1], p[1]))
        decay = jnp.broadcast_to(jnp.exp(final), (PAIR, PAIR))
        transfer = jnp.where(row2 == col2, decay, 0.0) - moved[:, :PAIR]
        added = gained - moved[:, PAIR:]
        halves = tuple(x[:, j : j + PAIR] for j in (0, PAIR) for x in both)
        out.append((fold(transfer), fold(added), running) + keep + halves)
    return out


def chunk_reads(pairs):
    size = pairs[0][0].shape[0]
    within = iota((size, size), 0) >= iota((size, size), 1)
    grids = []
    fronts = []
    for q, v, running, keep in pairs:
        centre = running[size // 2 : size // 2 + 1]
        read_from = q.astype(F32) * jnp.exp(running - centre)
        fronts.append(read_from * jnp.exp(centre))
        right = below(keep[0], keep[2]), below(keep[1], keep[3])
        grids.append(pair_grid(split(stack_pair(read_from)), right))
    out = []
    for (q, v, running, keep), grid, front in zip(pairs, grids, fronts):
        part = lambda i, j: jnp.where(
            within, grid[i * size : (i + 1) * size, j * size : (j + 1) * size], 0.0
        )
        read_keys = split(beside(part(0, 0), part(1, 0)))
        read_erase = split(beside(part(0, 1), part(1, 1)))
        values = stack_pair(v)
        here = mm(read_keys[0], values) + mm(read_keys[1], values)
        both = [stack_pair(beside(keep[i + 4], keep[i + 6])) for i in (0, 1)]
        taken = mm_ab(read_erase, both)
        out.append(split(front - taken[:, :PAIR]) + (here - taken[:, PAIR:],))
    return out


def normed(readout, ones):
    centred = readout - head_sum(readout, ones)
    variance = head_sum(centred * centred, ones)
    return centred * lax.rsqrt(variance + 1.0)


def fused_kernel(devices, columns, wide, pieces, q_ref, k_ref, v_ref, low_ref, rate_ref,
                 dup_ref, rup_ref, base_ref, gain_ref, weight_ref, out_ref, weights, own_ref,
                 running_ref, kept_ref, read_ref, here_ref, first_ref, first_add, both_ref, both_add,
                 mix_ref, give_buf, take_buf, start_buf, end_buf, own_sem, near_sem, far_send,
                 far_recv, side_send, side_recv, long_send, long_recv, pass_send, pass_recv,
                 give_send, give_recv, send_sem, recv_sem):
    me = lax.axis_index("sp")
    mine = lax.axis_index("dp")
    partner = mine + 1 - 2 * lax.rem(mine, 2)
    odd = lax.rem(me, 2)
    pair = me // 2
    side = me + 1 - 2 * odd
    long = me + 2 - 4 * lax.rem(pair, 2)
    width = q_ref.shape[1]
    blocks = width // wide
    chain = devices // 2
    others = columns // 2 - 1
    cols = weight_ref.shape[1]
    piece = weight_ref.shape[0] // (4 * pieces)
    has_left = pair > 0
    has_right = pair < chain - 1
    barrier = pltpu.get_barrier_semaphore()

    def greet(where):
        pl.semaphore_signal(barrier, inc=1, device_id=where, device_id_type=pl.DeviceIdType.MESH)

    def ahead_of(j):
        return lax.rem(mine + 2 * (j + 1), columns)

    def behind_of(j):
        return lax.rem(mine + columns - 2 * (j + 1), columns)

    def remote(src, dst, send, recv, where):
        return pltpu.make_async_remote_copy(
            src_ref=src, dst_ref=dst, send_sem=send, recv_sem=recv,
            device_id=where, device_id_type=pl.DeviceIdType.MESH,
        )

    greet({"dp": partner})
    greet({"sp": side})
    for j in range(others):
        greet({"dp": ahead_of(j)})

    @pl.when(has_left)
    def _():
        greet({"sp": me - 2})

    @pl.when(has_right)
    def _():
        greet({"sp": me + 2})

    own = pltpu.make_async_copy(weight_ref, weights.at[mine], own_sem)
    own.start()
    pl.semaphore_wait(
        barrier, 2 + others + jnp.minimum(pair, 1) + jnp.minimum(chain - 1 - pair, 1)
    )

    quarter = lax.rem(me, 4)
    side_quarter = quarter + 1 - 2 * odd
    long_quarter = lax.rem(quarter + 2, 4)
    last_quarter = 3 - quarter
    arrivals = (quarter, last_quarter, side_quarter, long_quarter)

    def rows(part, c):
        return pl.ds((part * pieces + c) * piece, piece)

    def far(j, part, c):
        at = rows(arrivals[part], c)
        return remote(
            weight_ref.at[at], weights.at[mine, at],
            far_send.at[j, part, c], far_recv.at[j, part, c], {"dp": ahead_of(j)},
        )

    def spread(j, c, send, recv, where):
        at = rows(quarter, c)
        spot = weights.at[behind_of(j), at]
        return remote(spot, spot, send.at[j, c], recv.at[j, c], {"sp": where})

    def aside(j, c):
        return spread(j, c, side_send, side_recv, side)

    def along(j, c):
        return spread(j, c, long_send, long_recv, long)

    def passed(j, part, c):
        spot = weights.at[behind_of(j), rows(arrivals[part], c)]
        return remote(
            spot, spot, pass_send.at[j, part, c], pass_recv.at[j, part, c], {"dp": partner},
        )

    near = remote(weight_ref, weights.at[mine], near_sem.at[0], near_sem.at[1], {"dp": partner})
    for part in range(2):
        for c in range(pieces):
            for j in range(others):
                far(j, part, c).start()
    near.start()

    def forward(part, c):
        for j in range(others):
            if part < 2:
                far(j, part, c).wait_recv()
            elif part == 2:
                aside(j, c).wait_recv()
            else:
                along(j, c).wait_recv()
            if part == 0:
                aside(j, c).start()
                along(j, c).start()
            passed(j, part, c).start()

    def lanes_of(g):
        return pl.ds(pl.multiple_of(g * wide, wide), wide)

    def cut(x, i):
        return x[:, i * PAIR : (i + 1) * PAIR]

    def cuts(x):
        return [cut(x, i) for i in range(wide // PAIR)]

    def give(b):
        return remote(
            give_buf.at[b], take_buf.at[b], give_send.at[b], give_recv.at[b], {"sp": side}
        )

    def copy(b):
        return remote(
            end_buf.at[b], start_buf.at[b], send_sem.at[b], recv_sem.at[b],
            {"sp": lax.rem(me + 2, devices)},
        )

    def make(b):
        at = lanes_of(b)
        squashed = jnp.tanh(low_ref[...].astype(F32)).astype(BF16)
        log_decay, rate = gates(
            squashed, rate_ref[...], dup_ref[:, at], rup_ref[:, at], base_ref[:, at]
        )
        pairs = list(zip(*map(cuts, (k_ref[:, at], v_ref[:, at], log_decay, rate))))
        parts = [beside(*part) for part in zip(*chunk_maps(pairs))]
        maps = below(parts[0], parts[1])
        own_ref[:, at] = maps
        give_buf[b] = maps.astype(BF16)
        running_ref[:, at] = parts[2]
        for i, part in enumerate(parts[3:]):
            kept_ref[i, :, at] = part
        give(b).start()

    def combine(b):
        at = lanes_of(b)
        give(b).wait_recv()
        own, taken = own_ref[:, at], take_buf[b].astype(F32)
        is_odd = iota(own.shape, 0) * 0 + odd == 1
        first, second = jnp.where(is_odd, taken, own), jnp.where(is_odd, own, taken)
        found = []
        for x, y in zip(cuts(first), cuts(second)):
            left = split(y[:HEAD])
            right = split(beside(stack_pair(x[:HEAD]), stack_pair(x[HEAD:])))
            found.append((mm_ab(left, right), y[HEAD:]))
        both = beside(*[x[:, :PAIR] for x, _ in found])
        added = beside(*[x[:, PAIR:] + y for x, y in found])
        both_ref[0, :, at], both_ref[1, :, at] = split(both)
        both_add[:, at] = added
        same = (iota((HEAD, wide), 1) % HEAD == iota((HEAD, wide), 0)).astype(F32)
        is_odd = is_odd[:HEAD]
        first_ref[0, :, at], first_ref[1, :, at] = split(jnp.where(is_odd, first[:HEAD], same))
        first_add[:, at] = jnp.where(is_odd, first[HEAD:], 0.0)

        @pl.when(jnp.logical_not(has_left) & has_right)
        def _():
            end_buf[b] = added.astype(BF16)
            copy(b).start()

    def apply(high, low, state):
        return mm(beside(high, low), below(state, state))

    def advance(b):
        at = lanes_of(b)
        copy(b).wait_recv()

        @pl.when(has_right)
        def _():
            high, low, start = both_ref[0, :, at], both_ref[1, :, at], start_buf[b]
            ends = [apply(h, l, stack_pair(x)) for h, l, x in zip(*map(cuts, (high, low, start)))]
            end_buf[b] = (beside(*ends) + both_add[:, at]).astype(BF16)
            copy(b).start()

    def prepare(b):
        at = lanes_of(b)
        kept = [cuts(kept_ref[j, :, at]) for j in range(kept_ref.shape[0])]
        keeps = list(zip(*kept))
        pairs = list(zip(*map(cuts, (q_ref[:, at], v_ref[:, at], running_ref[:, at])), keeps))
        high, low, here = [beside(*part) for part in zip(*chunk_reads(pairs))]
        read_ref[0, :, at], read_ref[1, :, at], here_ref[:, at] = high, low, here

    ones = head_ones(1.0 / HEAD)

    def read(b):
        at = lanes_of(b)
        high, low, start = first_ref[0, :, at], first_ref[1, :, at], start_buf[b]
        starts = [apply(h, l, stack_pair(x)) for h, l, x in zip(*map(cuts, (high, low, start)))]
        starts = [split(x + y) for x, y in zip(starts, cuts(first_add[:, at]))]
        high, low, here = read_ref[0, :, at], read_ref[1, :, at], here_ref[:, at]
        reads = []
        for h, l, x, (s_high, s_low) in zip(*map(cuts, (high, low, here)), starts):
            reads.append(apply(h, l, stack_pair(s_high)) + mm(h, stack_pair(s_low)) + x)
        centred = [x - head_sum(x, ones) for x in reads]
        spans = [head_sum(x * x, ones) for x in centred]
        mix = beside(*[x * lax.rsqrt(y + 1.0) for x, y in zip(centred, spans)])
        mix_ref[:, at] = (mix * gain_ref[:, at]).astype(BF16)

    @pl.when(jnp.logical_not(has_left))
    def _():
        start_buf[...] = jnp.zeros_like(start_buf)

    lag = jnp.maximum(pair - 1, 0)
    slots = 2 * blocks + max(chain - 2, 0)
    plan = [(2, [(0, 0)]), (3, [(0, 1)]), (5, [(0, 2)]), (6, [(2, 0), (3, 0)]), (7, [(0, 3), (2, 1), (3, 1)])]

    def slot(s, carry):
        @pl.when(s < blocks)
        def _():
            make(s)

        @pl.when(((s >= 1) & (s < blocks)) | (s == 2 * blocks - 1))
        def _():
            combine(jnp.minimum(s, blocks) - 1)

        b = s - blocks - lag
        live = (b >= 0) & (b < blocks)

        @pl.when(live & has_left)
        def _():
            advance(b)

        @pl.when((s >= blocks) & (s < 2 * blocks))
        def _():
            prepare(s - blocks)

        @pl.when(live)
        def _():
            read(b)

        for at, todo in plan:
            @pl.when(s == at)
            def _():
                for part, c in todo:
                    forward(part, c)

        return carry

    lax.fori_loop(0, slots, slot, 0)
    done = [x for _, todo in plan for x in todo]
    for c in range(pieces):
        for part in (0, 2, 3, 1):
            if (part, c) not in done:
                forward(part, c)

    def project(d):
        at = pl.ds(pl.multiple_of(d * cols, cols), cols)
        out_ref[:, at] = mm(mix_ref[...], weights[d]).astype(BF16)

    own.wait()
    project(mine)
    near.wait_recv()
    project(partner)
    for j in range(others):
        project(behind_of(j))
    for j in range(others):
        for part in range(4):
            for c in range(pieces):
                passed(j, part, c).wait_recv()
        project(lax.rem(partner + columns - 2 * (j + 1), columns))

    near.wait_send()
    for j in range(others):
        for part in range(4):
            for c in range(pieces):
                passed(j, part, c).wait_send()
        for c in range(pieces):
            aside(j, c).wait_send()
            along(j, c).wait_send()
            far(j, 0, c).wait_send()
            far(j, 1, c).wait_send()

    for b in range(blocks):
        give(b).wait_send()

    @pl.when(has_right)
    def _():
        for b in range(blocks):
            copy(b).wait_send()


def per_device(devices, columns, query_rows, key_rows, value_rows, decay_low, rate_low, decay_up,
               rate_up, decay_base, norm_gain, out_weight):
    q = query_rows[0]
    size, width = q.shape
    depth, cols = out_weight.shape
    wide = PAIR * math.gcd(width // PAIR, WIDE)
    blocks = width // wide
    pieces = 4
    others = columns // 2 - 1
    vmem = pl.BlockSpec(memory_space=pltpu.VMEM)
    dma = lambda *dims: pltpu.SemaphoreType.DMA(dims)
    out = pl.pallas_call(
        functools.partial(fused_kernel, devices, columns, wide, pieces),
        in_specs=[vmem] * 9 + [pl.BlockSpec(memory_space=pl.ANY)],
        out_specs=vmem,
        out_shape=jax.ShapeDtypeStruct((size, columns * cols), BF16),
        scratch_shapes=[
            pltpu.VMEM((columns, depth, cols), BF16),
            pltpu.VMEM((2 * HEAD, width), F32),
            pltpu.VMEM((size, width), F32),
            pltpu.VMEM((8, size, width), BF16),
            pltpu.VMEM((2, size, width), BF16),
            pltpu.VMEM((size, width), F32),
            pltpu.VMEM((2, HEAD, width), BF16),
            pltpu.VMEM((HEAD, width), F32),
            pltpu.VMEM((2, HEAD, width), BF16),
            pltpu.VMEM((HEAD, width), F32),
            pltpu.VMEM((size, width), BF16),
            pltpu.VMEM((blocks, 2 * HEAD, wide), BF16),
            pltpu.VMEM((blocks, 2 * HEAD, wide), BF16),
            pltpu.VMEM((blocks, HEAD, wide), BF16),
            pltpu.VMEM((blocks, HEAD, wide), BF16),
            pltpu.SemaphoreType.DMA,
            dma(2),
            dma(others, 2, pieces),
            dma(others, 2, pieces),
            dma(others, pieces),
            dma(others, pieces),
            dma(others, pieces),
            dma(others, pieces),
            dma(others, 4, pieces),
            dma(others, 4, pieces),
            dma(blocks),
            dma(blocks),
            dma(blocks),
            dma(blocks),
        ],
        compiler_params=pltpu.CompilerParams(collective_id=0, has_side_effects=True),
        name="fused_mixer",
    )(
        q, key_rows[0], value_rows[0], decay_low[0], rate_low[0], decay_up, rate_up,
        decay_base[None], norm_gain[None], out_weight,
    )
    return out[None]


def solution(mesh):
    in_specs = (
        P("dp", "sp", None),
        P("dp", "sp", None),
        P("dp", "sp", None),
        P("dp", "sp", None),
        P("dp", "sp", None),
        P(),
        P(),
        P(),
        P(),
        P(None, "dp"),
    )
    return jax.shard_map(
        functools.partial(per_device, mesh.shape["sp"], mesh.shape["dp"]),
        mesh=mesh, in_specs=in_specs, out_specs=P("dp", "sp", None), check_vma=False,
    )
```

time: 56.8 us -> 43 us (0.76)
  the two profiles are of different devices: /device:TPU:1 before, /device:TPU:27 now
where the time goes in v2:
time: 43 us; the launch traced here: 42.5 us
  Pallas kernels  40.6 us (94%)
  local copies, waits for them, and re-layouts  1.88 us (4%)
    pallas_call x1, Pallas kernels, per_device(): pl.pallas_call(functools.partial(fused_kernel, devices, columns, wide, pi...  40.6 us
    unnamed x1, local copies, waits for them, and re-layouts  1.88 us

profile of v2, /device:TPU:27, one launch (start us, length us, event | category | flops | bytes accessed | tf_op | source)
XLA Modules:
  0.0 42.5 jit_solution(15532417466908443233)
XLA Ops:
  0.0 40.6 %fused_mixer.1 = bf16[128,2048]{1,0:T(8,128)(2,1)} custom-call(bf16[128,2048]{1,0:T(8,128)(2,1)} %bitcast.9, bf16[128,2048]{1,0:T(8,128)(2,1)} %bitcast.10, bf16[128,2048]{1,0:T(8,128)(2,1)} %bitcast.11, bf16[128,128]{1,0:T(8,128)(2,1)} %bitcast.12, bf16[128,128]{1,0:T(8,128)(2,1)} %bitcast.13, bf16[128,2048]{1,0:T(8,128)(2,1)} %dup_ref.1, ...), custom_call_target="tpu_custom_call" | custom-call | tf_op jit(solution)/shard_map/fused_mixer/pallas_call | solution.py:521
  40.6 1.9 %copy.12 = bf16[1,128,2048]{2,1,0:T(8,128)(2,1)} copy(bf16[1,128,2048]{2,1,0:T(8,128)(2,1)} %bitcast.8) | data formatting | bytes 1048576

commit v3 on v2

--- a/solution.py
+++ b/solution.py
@@ -11,6 +11,7 @@
 HEAD = 64
 PAIR = 2 * HEAD
 WIDE = 4
+FINE = 16
 
 F32 = jnp.float32
 BF16 = jnp.bfloat16
@@ -71,6 +72,11 @@
 
 def head_sum(x, ones):
     return mm(beside(*split(x)), below(ones, ones))
+
+
+def crossed(x, y):
+    zero = jnp.zeros_like(x)
+    return below(beside(x, zero), beside(zero, y))
 
 
 def solve(parts, size):
@@ -126,10 +132,13 @@
     ones = head_ones(1.0)
     half = first_half((size, PAIR))
     runs = [mm(upto, below(*split(p[2]))) for p in pairs]
+    means = head_ones(1.0 / HEAD)
     sums = []
+    values = []
     for p in pairs:
         k = p[0].astype(F32)
         sums.append(head_sum(k * k, ones))
+        values.append(split(p[1].astype(F32) - mm(p[1], means)))
     made = []
     for (k, v, log_decay, rate), running, total in zip(pairs, runs, sums):
         k = k.astype(F32)
@@ -152,10 +161,9 @@
         )
 
     parts = []
-    for p, grid, (erase_from, _, _, centre, _) in zip(pairs, grids, made):
-        values = stack_pair(p[1])
+    for v, grid, (erase_from, _, _, centre, _) in zip(values, grids, made):
         keys = split(beside(part(grid, 0, 0), part(grid, 1, 0)))
-        carried = mm(keys[0], values) + mm(keys[1], values)
+        carried = mm_ab(keys, [stack_pair(x) for x in v])
         erase = erase_from * jnp.exp(centre)
         parts.append((part(grid, 0, 1), jnp.where(half, erase, swap(carried))))
         parts.append((part(grid, 1, 1), jnp.where(half, swap(erase), carried)))
@@ -165,8 +173,8 @@
     half2 = first_half((HEAD, PAIR))
     fold = lambda x: jnp.where(half2, x[:HEAD], x[HEAD:])
     out = []
-    for i, (p, keep, running, (_, key_to, erase_to, centre, final)) in enumerate(
-        zip(pairs, keeps, runs, made)
+    for i, (v, keep, running, (_, key_to, erase_to, centre, final)) in enumerate(
+        zip(values, keeps, runs, made)
     ):
         a, b = solved[2 * i], solved[2 * i + 1]
         both = split(beside(jnp.where(half, a, swap(b)), jnp.where(half, swap(a), b)))
@@ -174,12 +182,12 @@
         erase_end = split(erase_to * at_end)
         key_end = split(key_to * at_end)
         moved = mm_tn(below(*erase_end), below(both[0], both[0])) + mm_tn(erase_end[0], both[1])
-        gained = mm_tn(below(*key_end), below(p[1], p[1]))
+        gained = mm_tn(below(*key_end), below(v[0], v[0])) + mm_tn(key_end[0], v[1])
         decay = jnp.broadcast_to(jnp.exp(final), (PAIR, PAIR))
         transfer = jnp.where(row2 == col2, decay, 0.0) - moved[:, :PAIR]
         added = gained - moved[:, PAIR:]
         halves = tuple(x[:, j : j + PAIR] for j in (0, PAIR) for x in both)
-        out.append((fold(transfer), fold(added), running) + keep + halves)
+        out.append((fold(transfer), fold(added), running) + keep + halves + v)
     return out
 
 
@@ -188,35 +196,30 @@
     within = iota((size, size), 0) >= iota((size, size), 1)
     grids = []
     fronts = []
-    for q, v, running, keep in pairs:
+    for q, running, keep in pairs:
         centre = running[size // 2 : size // 2 + 1]
         read_from = q.astype(F32) * jnp.exp(running - centre)
         fronts.append(read_from * jnp.exp(centre))
         right = below(keep[0], keep[2]), below(keep[1], keep[3])
         grids.append(pair_grid(split(stack_pair(read_from)), right))
     out = []
-    for (q, v, running, keep), grid, front in zip(pairs, grids, fronts):
+    for (_, _, keep), grid, front in zip(pairs, grids, fronts):
         part = lambda i, j: jnp.where(
             within, grid[i * size : (i + 1) * size, j * size : (j + 1) * size], 0.0
         )
         read_keys = split(beside(part(0, 0), part(1, 0)))
         read_erase = split(beside(part(0, 1), part(1, 1)))
-        values = stack_pair(v)
-        here = mm(read_keys[0], values) + mm(read_keys[1], values)
+        here = mm_ab(read_keys, [stack_pair(x) for x in keep[8:]])
         both = [stack_pair(beside(keep[i + 4], keep[i + 6])) for i in (0, 1)]
         taken = mm_ab(read_erase, both)
         out.append(split(front - taken[:, :PAIR]) + (here - taken[:, PAIR:],))
     return out
 
 
-def normed(readout, ones):
-    centred = readout - head_sum(readout, ones)
-    variance = head_sum(centred * centred, ones)
-    return centred * lax.rsqrt(variance + 1.0)
-
-
-def fused_kernel(devices, columns, wide, pieces, q_ref, k_ref, v_ref, low_ref, rate_ref,
-                 dup_ref, rup_ref, base_ref, gain_ref, weight_ref, out_ref, weights, own_ref,
+def fused_kernel(devices, columns, wide, pieces, q_hbm, k_hbm, v_hbm, low_hbm, rate_hbm,
+                 dup_hbm, rup_hbm, base_hbm, gain_hbm, weight_ref, out_ref, q_ref, k_ref, v_ref,
+                 low_ref, rate_ref, dup_ref, rup_ref, base_ref, gain_ref, in_sem, sums_ref, weights,
+                 own_ref,
                  running_ref, kept_ref, read_ref, here_ref, first_ref, first_add, both_ref, both_add,
                  mix_ref, give_buf, take_buf, start_buf, end_buf, own_sem, near_sem, far_send,
                  far_recv, side_send, side_recv, long_send, long_recv, pass_send, pass_recv,
@@ -266,6 +269,13 @@
     def _():
         greet({"sp": me + 2})
 
+    inputs = [
+        (low_hbm, low_ref), (rate_hbm, rate_ref), (base_hbm, base_ref), (dup_hbm, dup_ref),
+        (rup_hbm, rup_ref), (k_hbm, k_ref), (v_hbm, v_ref), (q_hbm, q_ref), (gain_hbm, gain_ref),
+    ]
+    loads = [pltpu.make_async_copy(x, y, in_sem.at[i]) for i, (x, y) in enumerate(inputs)]
+    for load in loads:
+        load.start()
     own = pltpu.make_async_copy(weight_ref, weights.at[mine], own_sem)
     own.start()
     pl.semaphore_wait(
@@ -321,9 +331,12 @@
             else:
                 along(j, c).wait_recv()
             if part == 0:
-                aside(j, c).start()
                 along(j, c).start()
             passed(j, part, c).start()
+
+    def lend(c):
+        for j in range(others):
+            aside(j, c).start()
 
     def lanes_of(g):
         return pl.ds(pl.multiple_of(g * wide, wide), wide)
@@ -404,7 +417,7 @@
         at = lanes_of(b)
         kept = [cuts(kept_ref[j, :, at]) for j in range(kept_ref.shape[0])]
         keeps = list(zip(*kept))
-        pairs = list(zip(*map(cuts, (q_ref[:, at], v_ref[:, at], running_ref[:, at])), keeps))
+        pairs = list(zip(*map(cuts, (q_ref[:, at], running_ref[:, at])), keeps))
         high, low, here = [beside(*part) for part in zip(*chunk_reads(pairs))]
         read_ref[0, :, at], read_ref[1, :, at], here_ref[:, at] = high, low, here
 
@@ -419,20 +432,40 @@
         reads = []
         for h, l, x, (s_high, s_low) in zip(*map(cuts, (high, low, here)), starts):
             reads.append(apply(h, l, stack_pair(s_high)) + mm(h, stack_pair(s_low)) + x)
-        centred = [x - head_sum(x, ones) for x in reads]
-        spans = [head_sum(x * x, ones) for x in centred]
-        mix = beside(*[x * lax.rsqrt(y + 1.0) for x, y in zip(centred, spans)])
-        mix_ref[:, at] = (mix * gain_ref[:, at]).astype(BF16)
+        spans = [head_sum(x * x, ones) for x in reads]
+        mix = beside(*[x * lax.rsqrt(y + 1.0) for x, y in zip(reads, spans)])
+        mix = (mix * gain_ref[:, at]).astype(BF16)
+        mix_ref[:, at] = mix
+        for i, d in enumerate((mine, partner)):
+            sums_ref[i] += mm(mix, weights[d, at])
 
     @pl.when(jnp.logical_not(has_left))
     def _():
         start_buf[...] = jnp.zeros_like(start_buf)
 
+    sums_ref[...] = jnp.zeros_like(sums_ref)
+    for load in loads:
+        load.wait()
+
     lag = jnp.maximum(pair - 1, 0)
     slots = 2 * blocks + max(chain - 2, 0)
-    plan = [(2, [(0, 0)]), (3, [(0, 1)]), (5, [(0, 2)]), (6, [(2, 0), (3, 0)]), (7, [(0, 3), (2, 1), (3, 1)])]
+    plan = [
+        (1, [(0, 0)]),
+        (2, [(0, 1), (-1, 0)]),
+        (blocks - 1, [(0, 2), (-1, 1)]),
+    ]
+    early = [(blocks + 1, [(0, 3), (-1, 2)]), (blocks + 2, [(-1, 3)]), (2 * blocks + 1, [(3, 0), (3, 1), (2, 0), (3, 2), (2, 1), (1, 0), (3, 3), (2, 2), (2, 3), (1, 1)])]
 
     def slot(s, carry):
+        def pump(which):
+            for at, todo in which:
+                @pl.when(s == at)
+                def _():
+                    for part, c in todo:
+                        (lend if part < 0 else functools.partial(forward, part))(c)
+
+        pump(early)
+
         @pl.when(s < blocks)
         def _():
             make(s)
@@ -452,22 +485,22 @@
         def _():
             prepare(s - blocks)
 
+        @pl.when(s == blocks)
+        def _():
+            own.wait()
+            near.wait_recv()
+
         @pl.when(live)
         def _():
             read(b)
 
-        for at, todo in plan:
-            @pl.when(s == at)
-            def _():
-                for part, c in todo:
-                    forward(part, c)
-
+        pump(plan)
         return carry
 
     lax.fori_loop(0, slots, slot, 0)
-    done = [x for _, todo in plan for x in todo]
+    done = [x for at, todo in plan + early if at < slots for x in todo]
     for c in range(pieces):
-        for part in (0, 2, 3, 1):
+        for part in (0, 3, 2, 1):
             if (part, c) not in done:
                 forward(part, c)
 
@@ -475,10 +508,9 @@
         at = pl.ds(pl.multiple_of(d * cols, cols), cols)
         out_ref[:, at] = mm(mix_ref[...], weights[d]).astype(BF16)
 
-    own.wait()
-    project(mine)
-    near.wait_recv()
-    project(partner)
+    for i, d in enumerate((mine, partner)):
+        at = pl.ds(pl.multiple_of(d * cols, cols), cols)
+        out_ref[:, at] = sums_ref[i].astype(BF16)
     for j in range(others):
         project(behind_of(j))
     for j in range(others):
@@ -520,14 +552,25 @@
     dma = lambda *dims: pltpu.SemaphoreType.DMA(dims)
     out = pl.pallas_call(
         functools.partial(fused_kernel, devices, columns, wide, pieces),
-        in_specs=[vmem] * 9 + [pl.BlockSpec(memory_space=pl.ANY)],
+        in_specs=[pl.BlockSpec(memory_space=pl.ANY)] * 10,
         out_specs=vmem,
         out_shape=jax.ShapeDtypeStruct((size, columns * cols), BF16),
         scratch_shapes=[
+            pltpu.VMEM((size, width), BF16),
+            pltpu.VMEM((size, width), BF16),
+            pltpu.VMEM((size, width), BF16),
+            pltpu.VMEM(decay_low.shape[1:], BF16),
+            pltpu.VMEM(rate_low.shape[1:], BF16),
+            pltpu.VMEM(decay_up.shape, BF16),
+            pltpu.VMEM(rate_up.shape, BF16),
+            pltpu.VMEM((1, width), F32),
+            pltpu.VMEM((1, width), F32),
+            dma(9),
+            pltpu.VMEM((2, size, cols), F32),
             pltpu.VMEM((columns, depth, cols), BF16),
             pltpu.VMEM((2 * HEAD, width), F32),
             pltpu.VMEM((size, width), F32),
-            pltpu.VMEM((8, size, width), BF16),
+            pltpu.VMEM((10, size, width), BF16),
             pltpu.VMEM((2, size, width), BF16),
             pltpu.VMEM((size, width), F32),
             pltpu.VMEM((2, HEAD, width), BF16),

time: 43 us -> 40.1 us (0.933)
  Pallas kernels: 40.6 us -> 37.9 us
    pallas_call x1, Pallas kernels: 40.6 us -> 37.9 us  [per_device(): pl.pallas_call(functools.partial(fused_kernel, devices, columns, wide, pi...]
where the time goes in v3:
time: 40.1 us; the launch traced here: 39.8 us
  Pallas kernels  37.9 us (95%)
  local copies, waits for them, and re-layouts  1.88 us (5%)
    pallas_call x1, Pallas kernels, per_device(): pl.pallas_call(functools.partial(fused_kernel, devices, columns, wide, pi...  37.9 us
    unnamed x1, local copies, waits for them, and re-layouts  1.88 us

profile of v3, /device:TPU:27, one launch (start us, length us, event | category | flops | bytes accessed | tf_op | source)
XLA Modules:
  0.0 39.8 jit_solution(15792680342230282286)
XLA Ops:
  0.0 37.9 %fused_mixer.1 = bf16[128,2048]{1,0:T(8,128)(2,1)} custom-call(bf16[128,2048]{1,0:T(8,128)(2,1)} %bitcast.9, bf16[128,2048]{1,0:T(8,128)(2,1)} %bitcast.10, bf16[128,2048]{1,0:T(8,128)(2,1)} %bitcast.11, bf16[128,128]{1,0:T(8,128)(2,1)} %bitcast.12, bf16[128,128]{1,0:T(8,128)(2,1)} %bitcast.13, bf16[128,2048]{1,0:T(8,128)(2,1)} %dup_hbm.1, ...), custom_call_target="tpu_custom_call" | custom-call | tf_op jit(solution)/shard_map/fused_mixer/pallas_call | solution.py:553
  37.9 1.9 %copy.12 = bf16[1,128,2048]{2,1,0:T(8,128)(2,1)} copy(bf16[1,128,2048]{2,1,0:T(8,128)(2,1)} %bitcast.8) | data formatting | bytes 1048576

commit v4 on v3

--- a/solution.py
+++ b/solution.py
@@ -352,11 +352,17 @@
             give_buf.at[b], take_buf.at[b], give_send.at[b], give_recv.at[b], {"sp": side}
         )
 
-    def copy(b):
+    def copy(b, i):
         return remote(
-            end_buf.at[b], start_buf.at[b], send_sem.at[b], recv_sem.at[b],
+            end_buf.at[b, i], start_buf.at[b, i], send_sem.at[b, i], recv_sem.at[b, i],
             {"sp": lax.rem(me + 2, devices)},
         )
+
+    shares = end_buf.shape[1]
+    share = wide // shares
+
+    def start_of(b):
+        return beside(*[start_buf[b, i] for i in range(shares)])
 
     def make(b):
         at = lanes_of(b)
@@ -396,22 +402,27 @@
 
         @pl.when(jnp.logical_not(has_left) & has_right)
         def _():
-            end_buf[b] = added.astype(BF16)
-            copy(b).start()
+            for i in range(shares):
+                end_buf[b, i] = added[:, i * share : (i + 1) * share].astype(BF16)
+                copy(b, i).start()
 
     def apply(high, low, state):
         return mm(beside(high, low), below(state, state))
 
     def advance(b):
-        at = lanes_of(b)
-        copy(b).wait_recv()
-
-        @pl.when(has_right)
-        def _():
-            high, low, start = both_ref[0, :, at], both_ref[1, :, at], start_buf[b]
-            ends = [apply(h, l, stack_pair(x)) for h, l, x in zip(*map(cuts, (high, low, start)))]
-            end_buf[b] = (beside(*ends) + both_add[:, at]).astype(BF16)
-            copy(b).start()
+        for i in range(shares):
+            copy(b, i).wait_recv()
+
+            @pl.when(has_right)
+            def _():
+                at = pl.ds(pl.multiple_of(b * wide + i * share, share), share)
+                high, low, start = both_ref[0, :, at], both_ref[1, :, at], start_buf[b, i]
+                ends = []
+                for j in range(share // PAIR):
+                    h, l, x = cut(high, j), cut(low, j), cut(start, j)
+                    ends.append(apply(h, l, stack_pair(x)))
+                end_buf[b, i] = (beside(*ends) + both_add[:, at]).astype(BF16)
+                copy(b, i).start()
 
     def prepare(b):
         at = lanes_of(b)
@@ -425,7 +436,7 @@
 
     def read(b):
         at = lanes_of(b)
-        high, low, start = first_ref[0, :, at], first_ref[1, :, at], start_buf[b]
+        high, low, start = first_ref[0, :, at], first_ref[1, :, at], start_of(b)
         starts = [apply(h, l, stack_pair(x)) for h, l, x in zip(*map(cuts, (high, low, start)))]
         starts = [split(x + y) for x, y in zip(starts, cuts(first_add[:, at]))]
         high, low, here = read_ref[0, :, at], read_ref[1, :, at], here_ref[:, at]
@@ -454,7 +465,7 @@
         (2, [(0, 1), (-1, 0)]),
         (blocks - 1, [(0, 2), (-1, 1)]),
     ]
-    early = [(blocks + 1, [(0, 3), (-1, 2)]), (blocks + 2, [(-1, 3)]), (2 * blocks + 1, [(3, 0), (3, 1), (2, 0), (3, 2), (2, 1), (1, 0), (3, 3), (2, 2), (2, 3), (1, 1)])]
+    early = [(blocks + 1, [(0, 3), (-1, 2)]), (blocks + 2, [(-1, 3)]), (2 * blocks, [(3, 0), (3, 1), (2, 0), (3, 2), (2, 1), (1, 0)]), (2 * blocks + 1, [(3, 3), (2, 2), (2, 3), (1, 1)])]
 
     def slot(s, carry):
         def pump(which):
@@ -536,7 +547,12 @@
     @pl.when(has_right)
     def _():
         for b in range(blocks):
-            copy(b).wait_send()
+            for i in range(shares):
+                copy(b, i).wait_send()
+
+
+def pin(x):
+    return pltpu.with_memory_space_constraint(x, pltpu.HBM)
 
 
 def per_device(devices, columns, query_rows, key_rows, value_rows, decay_low, rate_low, decay_up,
@@ -546,6 +562,7 @@
     depth, cols = out_weight.shape
     wide = PAIR * math.gcd(width // PAIR, WIDE)
     blocks = width // wide
+    shares = math.gcd(wide // PAIR, 2)
     pieces = 4
     others = columns // 2 - 1
     vmem = pl.BlockSpec(memory_space=pltpu.VMEM)
@@ -580,8 +597,8 @@
             pltpu.VMEM((size, width), BF16),
             pltpu.VMEM((blocks, 2 * HEAD, wide), BF16),
             pltpu.VMEM((blocks, 2 * HEAD, wide), BF16),
-            pltpu.VMEM((blocks, HEAD, wide), BF16),
-            pltpu.VMEM((blocks, HEAD, wide), BF16),
+            pltpu.VMEM((blocks, shares, HEAD, wide // shares), BF16),
+            pltpu.VMEM((blocks, shares, HEAD, wide // shares), BF16),
             pltpu.SemaphoreType.DMA,
             dma(2),
             dma(others, 2, pieces),
@@ -594,14 +611,14 @@
             dma(others, 4, pieces),
             dma(blocks),
             dma(blocks),
-            dma(blocks),
-            dma(blocks),
+            dma(blocks, shares),
+            dma(blocks, shares),
         ],
-        compiler_params=pltpu.CompilerParams(collective_id=0, has_side_effects=True),
+        compiler_params=pltpu.CompilerParams(collective_id=0, has_side_effects=True, vmem_limit_bytes=45 * 2**20),
         name="fused_mixer",
     )(
-        q, key_rows[0], value_rows[0], decay_low[0], rate_low[0], decay_up, rate_up,
-        decay_base[None], norm_gain[None], out_weight,
+        *map(pin, (q, key_rows[0], value_rows[0], decay_low[0], rate_low[0], decay_up, rate_up,
+        decay_base[None], norm_gain[None], out_weight)),
     )
     return out[None]
 

time: 40.1 us -> 37.9 us (0.945)
  local copies, waits for them, and re-layouts: 1.88 us -> 0.8 us
  Pallas kernels: 37.9 us -> 37 us
    unnamed x1, local copies, waits for them, and re-layouts: 1.88 us -> 0.8 us
    pallas_call x1, Pallas kernels: 37.9 us -> 37 us  [per_device(): pl.pallas_call(functools.partial(fused_kernel, devices, columns, wide, pi...]
where the time goes in v4:
time: 37.9 us; the launch traced here: 37.8 us
  Pallas kernels  37 us (98%)
  local copies, waits for them, and re-layouts  0.8 us (2%)
    pallas_call x1, Pallas kernels, per_device(): pl.pallas_call(functools.partial(fused_kernel, devices, columns, wide, pi...  37 us
    unnamed x1, local copies, waits for them, and re-layouts  0.8 us

profile of v4, /device:TPU:27, one launch (start us, length us, event | category | flops | bytes accessed | tf_op | source)
XLA Modules:
  0.0 37.8 jit_solution(12702162020342525723)
XLA Ops:
  0.0 37.0 %fused_mixer.1 = bf16[128,2048]{1,0:T(8,128)(2,1)S(1)} custom-call(bf16[128,2048]{1,0:T(8,128)(2,1)} %bitcast.9, bf16[128,2048]{1,0:T(8,128)(2,1)} %bitcast.10, bf16[128,2048]{1,0:T(8,128)(2,1)} %bitcast.11, bf16[128,128]{1,0:T(8,128)(2,1)} %bitcast.12, bf16[128,128]{1,0:T(8,128)(2,1)} %bitcast.13, bf16[128,2048]{1,0:T(8,128)(2,1)} %dup_hbm.1, ...), custom_call_target="tpu_custom_call" | custom-call | tf_op jit(solution)/shard_map/fused_mixer/pallas_call | solution.py:570
  37.0 0.8 %copy.12 = bf16[1,128,2048]{2,1,0:T(8,128)(2,1)} copy(bf16[1,128,2048]{2,1,0:T(8,128)(2,1)S(1)} %bitcast.8) | data formatting | bytes 1048576

commit v5 on v4

--- a/solution.py
+++ b/solution.py
@@ -12,6 +12,7 @@
 PAIR = 2 * HEAD
 WIDE = 4
 FINE = 16
+FINE = 16
 
 F32 = jnp.float32
 BF16 = jnp.bfloat16
@@ -79,31 +80,54 @@
     return below(beside(x, zero), beside(zero, y))
 
 
+def crossed(x, y):
+    zero = jnp.zeros_like(x)
+    return below(beside(x, zero), beside(zero, y))
+
+
 def solve(parts, size):
     row = iota((size, size), 0)
     col = iota((size, size), 1)
-    whole = [beside(z, y) for z, y in parts]
+
+    def picked(x, block):
+        keep = (row // (2 * block) == col // (2 * block)) & (row // block != col // block)
+        return jnp.where(keep, x, jnp.zeros_like(x))
+
+    small = [jnp.where(row // FINE == col // FINE, z, 0.0) for z, _ in parts]
     block = 1
+    while block < FINE:
+        high = [x.astype(BF16) for x in small]
+        steps = []
+        for x, y in zip(high[::2], high[1::2]):
+            both = mm(beside(picked(x, block), picked(y, block)), crossed(x, y))
+            steps += [both[:, :size], both[:, size:]]
+        small = [x - step for x, step in zip(small, steps)]
+        block *= 2
+    whole = []
+    for (z, y), x in zip(parts, small):
+        x = x.astype(BF16)
+        both = beside(z, y)
+        whole.append(both - mm(beside(x, x), below(*split(both))))
     while block < size:
-        last = 2 * block == size
-        pick = (row // (2 * block) == col // (2 * block)) & (row // block != col // block)
-        fine = block % 16 != 0
-        spans = [(0, size)] if fine else [(r + block, r + 2 * block) for r in range(0, size, 2 * block)]
+        keep = (row // (2 * block) == col // (2 * block)) & (row // block != col // block)
         found = []
         for x in whole:
-            high, low = split(x)
-            move = jnp.where(pick, high[:, :size], jnp.zeros_like(high[:, :size]))
-            move = move if fine else below(*[move[a:b] for a, b in spans])
-            if last:
-                x, high, low = x[:, size:], high[:, size:], low[:, size:]
-            step = mm(beside(move, move), below(high, low))
-            if fine:
-                found.append(x - step)
-            else:
-                rows = []
-                for i, (a, b) in enumerate(spans):
-                    rows += [x[a - block : a], x[a:b] - step[i * block : (i + 1) * block]]
-                found.append(below(*rows))
+            first = size if 2 * block == size else 0
+            moves, high, low, evens, odds = [], [], [], [], []
+            for r in range(0, size, 2 * block):
+                m, n = r + block, r + 2 * block
+                z = x[m:n, :size].astype(BF16)
+                moves.append(jnp.where(keep[m:n], z, jnp.zeros_like(z)))
+                evens.append(x[r:m, first:])
+                odds.append(x[m:n, first:])
+                for parts_of, piece in zip((high, low), split(evens[-1])):
+                    parts_of += [piece, jnp.zeros_like(piece)]
+            move = below(*moves)
+            step = mm(beside(move, move), below(*high, *low))
+            rows = []
+            for i, (even, odd) in enumerate(zip(evens, odds)):
+                rows += [even, odd - step[i * block : (i + 1) * block]]
+            found.append(below(*rows))
         whole = found
         block *= 2
     return whole
@@ -137,7 +161,7 @@
     values = []
     for p in pairs:
         k = p[0].astype(F32)
-        sums.append(head_sum(k * k, ones))
+        sums.append(mm((k * k).astype(BF16), ones))
         values.append(split(p[1].astype(F32) - mm(p[1], means)))
     made = []
     for (k, v, log_decay, rate), running, total in zip(pairs, runs, sums):
@@ -173,21 +197,19 @@
     half2 = first_half((HEAD, PAIR))
     fold = lambda x: jnp.where(half2, x[:HEAD], x[HEAD:])
     out = []
-    for i, (v, keep, running, (_, key_to, erase_to, centre, final)) in enumerate(
+    for i, (v, keep, running, (_, _, _, centre, final)) in enumerate(
         zip(values, keeps, runs, made)
     ):
         a, b = solved[2 * i], solved[2 * i + 1]
         both = split(beside(jnp.where(half, a, swap(b)), jnp.where(half, swap(a), b)))
-        at_end = jnp.exp(final - centre)
-        erase_end = split(erase_to * at_end)
-        key_end = split(key_to * at_end)
-        moved = mm_tn(below(*erase_end), below(both[0], both[0])) + mm_tn(erase_end[0], both[1])
-        gained = mm_tn(below(*key_end), below(v[0], v[0])) + mm_tn(key_end[0], v[1])
-        decay = jnp.broadcast_to(jnp.exp(final), (PAIR, PAIR))
-        transfer = jnp.where(row2 == col2, decay, 0.0) - moved[:, :PAIR]
-        added = gained - moved[:, PAIR:]
+        at_end = fold(jnp.transpose(jnp.broadcast_to(jnp.exp(final - centre), (PAIR, PAIR))))
+        moved = mm_tn(below(*keep[2:]), below(both[0], both[0])) + mm_tn(keep[2], both[1])
+        gained = mm_tn(below(*keep[:2]), below(v[0], v[0])) + mm_tn(keep[0], v[1])
+        decay = jnp.where(row2 == col2, jnp.broadcast_to(jnp.exp(final), (PAIR, PAIR)), 0.0)
+        transfer = fold(decay) - fold(moved[:, :PAIR]) * at_end
+        added = fold(gained - moved[:, PAIR:]) * at_end
         halves = tuple(x[:, j : j + PAIR] for j in (0, PAIR) for x in both)
-        out.append((fold(transfer), fold(added), running) + keep + halves + v)
+        out.append((transfer, added, running) + keep + halves + v)
     return out
 
 
@@ -256,19 +278,6 @@
             device_id=where, device_id_type=pl.DeviceIdType.MESH,
         )
 
-    greet({"dp": partner})
-    greet({"sp": side})
-    for j in range(others):
-        greet({"dp": ahead_of(j)})
-
-    @pl.when(has_left)
-    def _():
-        greet({"sp": me - 2})
-
-    @pl.when(has_right)
-    def _():
-        greet({"sp": me + 2})
-
     inputs = [
         (low_hbm, low_ref), (rate_hbm, rate_ref), (base_hbm, base_ref), (dup_hbm, dup_ref),
         (rup_hbm, rup_ref), (k_hbm, k_ref), (v_hbm, v_ref), (q_hbm, q_ref), (gain_hbm, gain_ref),
@@ -276,8 +285,20 @@
     loads = [pltpu.make_async_copy(x, y, in_sem.at[i]) for i, (x, y) in enumerate(inputs)]
     for load in loads:
         load.start()
+    greet({"dp": partner})
+    greet({"sp": side})
+    for j in range(others):
+        greet({"dp": ahead_of(j)})
+
+    @pl.when(has_left)
+    def _():
+        greet({"sp": me - 2})
+
+    @pl.when(has_right)
+    def _():
+        greet({"sp": me + 2})
+
     own = pltpu.make_async_copy(weight_ref, weights.at[mine], own_sem)
-    own.start()
     pl.semaphore_wait(
         barrier, 2 + others + jnp.minimum(pair, 1) + jnp.minimum(chain - 1 - pair, 1)
     )
@@ -320,7 +341,6 @@
         for c in range(pieces):
             for j in range(others):
                 far(j, part, c).start()
-    near.start()
 
     def forward(part, c):
         for j in range(others):
@@ -454,9 +474,11 @@
     def _():
         start_buf[...] = jnp.zeros_like(start_buf)
 
-    sums_ref[...] = jnp.zeros_like(sums_ref)
+    sums_ref[:2] = jnp.zeros((2, *sums_ref.shape[1:]), F32)
     for load in loads:
         load.wait()
+    own.start()
+    near.start()
 
     lag = jnp.maximum(pair - 1, 0)
     slots = 2 * blocks + max(chain - 2, 0)
@@ -465,11 +487,21 @@
         (2, [(0, 1), (-1, 0)]),
         (blocks - 1, [(0, 2), (-1, 1)]),
     ]
-    early = [(blocks + 1, [(0, 3), (-1, 2)]), (blocks + 2, [(-1, 3)]), (2 * blocks, [(3, 0), (3, 1), (2, 0), (3, 2), (2, 1), (1, 0)]), (2 * blocks + 1, [(3, 3), (2, 2), (2, 3), (1, 1)])]
+    early = [
+        (blocks + 1, [(0, 3), (-1, 2)]),
+        (blocks + 2, [(-1, 3)]),
+        (2 * blocks, [(3, 0), (3, 1), (2, 0), (3, 2), (2, 1), (1, 0)]),
+    ]
+    done = [x for at, todo in plan + early if at < slots - 1 for x in todo]
+    head = (blocks - 1) * wide
+    far_columns = [
+        d for j in range(others)
+        for d in (behind_of(j), lax.rem(partner + columns - 2 * (j + 1), columns))
+    ]
 
     def slot(s, carry):
         def pump(which):
-            for at, todo in which:
+            for at, todo in [x for x in which if x[0] < slots - 1]:
                 @pl.when(s == at)
                 def _():
                     for part, c in todo:
@@ -477,6 +509,19 @@
 
         pump(early)
 
+        @pl.when(s == slots - 1)
+        def _():
+            for c in range(pieces):
+                for part in (3, 2, 1, 0):
+                    if (part, c) not in done:
+                        forward(part, c)
+            for j in range(others):
+                for part in range(4):
+                    for c in range(pieces):
+                        passed(j, part, c).wait_recv()
+            for i, d in enumerate(far_columns):
+                sums_ref[2 + i] = mm(mix_ref[:, :head], weights[d, :head])
+
         @pl.when(s < blocks)
         def _():
             make(s)
@@ -509,26 +554,14 @@
         return carry
 
     lax.fori_loop(0, slots, slot, 0)
-    done = [x for at, todo in plan + early if at < slots for x in todo]
-    for c in range(pieces):
-        for part in (0, 3, 2, 1):
-            if (part, c) not in done:
-                forward(part, c)
-
-    def project(d):
-        at = pl.ds(pl.multiple_of(d * cols, cols), cols)
-        out_ref[:, at] = mm(mix_ref[...], weights[d]).astype(BF16)
+    def columns_of(d):
+        return pl.ds(pl.multiple_of(d * cols, cols), cols)
 
     for i, d in enumerate((mine, partner)):
-        at = pl.ds(pl.multiple_of(d * cols, cols), cols)
-        out_ref[:, at] = sums_ref[i].astype(BF16)
-    for j in range(others):
-        project(behind_of(j))
-    for j in range(others):
-        for part in range(4):
-            for c in range(pieces):
-                passed(j, part, c).wait_recv()
-        project(lax.rem(partner + columns - 2 * (j + 1), columns))
+        out_ref[:, columns_of(d)] = sums_ref[i].astype(BF16)
+    for i, d in enumerate(far_columns):
+        rest = mm(mix_ref[:, head:], weights[d, head:])
+        out_ref[:, columns_of(d)] = (sums_ref[2 + i] + rest).astype(BF16)
 
     near.wait_send()
     for j in range(others):
@@ -583,7 +616,7 @@
             pltpu.VMEM((1, width), F32),
             pltpu.VMEM((1, width), F32),
             dma(9),
-            pltpu.VMEM((2, size, cols), F32),
+            pltpu.VMEM((columns, size, cols), F32),
             pltpu.VMEM((columns, depth, cols), BF16),
             pltpu.VMEM((2 * HEAD, width), F32),
             pltpu.VMEM((size, width), F32),

time: 37.9 us -> 37.3 us (0.984); the launches traced: 37.8 us -> 36.5 us
  Pallas kernels: 37 us -> 35.7 us
    pallas_call x1, Pallas kernels: 37 us -> 35.7 us  [per_device(): pl.pallas_call(functools.partial(fused_kernel, devices, columns, wide, pi...]
where the time goes in v5:
time: 37.3 us; the launch traced here: 36.5 us
  Pallas kernels  35.7 us (96%)
  local copies, waits for them, and re-layouts  0.8 us (2%)
    pallas_call x1, Pallas kernels, per_device(): pl.pallas_call(functools.partial(fused_kernel, devices, columns, wide, pi...  35.7 us
    unnamed x1, local copies, waits for them, and re-layouts  0.8 us

profile of v5, /device:TPU:27, one launch (start us, length us, event | category | flops | bytes accessed | tf_op | source)
XLA Modules:
  0.0 36.5 jit_solution(17070750879935668719)
XLA Ops:
  0.0 35.7 %fused_mixer.1 = bf16[128,2048]{1,0:T(8,128)(2,1)S(1)} custom-call(bf16[128,2048]{1,0:T(8,128)(2,1)} %bitcast.9, bf16[128,2048]{1,0:T(8,128)(2,1)} %bitcast.10, bf16[128,2048]{1,0:T(8,128)(2,1)} %bitcast.11, bf16[128,128]{1,0:T(8,128)(2,1)} %bitcast.12, bf16[128,128]{1,0:T(8,128)(2,1)} %bitcast.13, bf16[128,2048]{1,0:T(8,128)(2,1)} %dup_hbm.1, ...), custom_call_target="tpu_custom_call" | custom-call | tf_op jit(solution)/shard_map/fused_mixer/pallas_call | solution.py:603
  35.7 0.8 %copy.12 = bf16[1,128,2048]{2,1,0:T(8,128)(2,1)} copy(bf16[1,128,2048]{2,1,0:T(8,128)(2,1)S(1)} %bitcast.8) | data formatting | bytes 1048576

commit v6 on v5

--- a/solution.py
+++ b/solution.py
@@ -484,12 +484,11 @@
     slots = 2 * blocks + max(chain - 2, 0)
     plan = [
         (1, [(0, 0)]),
-        (2, [(0, 1), (-1, 0)]),
-        (blocks - 1, [(0, 2), (-1, 1)]),
+        (2, [(0, 1)]),
+        (blocks - 1, [(-1, 0), (-1, 1), (0, 2)]),
     ]
     early = [
-        (blocks + 1, [(0, 3), (-1, 2)]),
-        (blocks + 2, [(-1, 3)]),
+        (blocks + 1, [(0, 3), (-1, 2), (-1, 3)]),
         (2 * blocks, [(3, 0), (3, 1), (2, 0), (3, 2), (2, 1), (1, 0)]),
     ]
     done = [x for at, todo in plan + early if at < slots - 1 for x in todo]
@@ -515,11 +514,11 @@
                 for part in (3, 2, 1, 0):
                     if (part, c) not in done:
                         forward(part, c)
-            for j in range(others):
-                for part in range(4):
-                    for c in range(pieces):
-                        passed(j, part, c).wait_recv()
             for i, d in enumerate(far_columns):
+                if i % 2 == 1:
+                    for part in range(4):
+                        for c in range(pieces):
+                            passed(i // 2, part, c).wait_recv()
                 sums_ref[2 + i] = mm(mix_ref[:, :head], weights[d, :head])
 
         @pl.when(s < blocks)

time: 37.3 us -> 37.1 us (level)
  no operation moved by 1% of the time
where the time goes in v6:
time: 37.1 us; the launch traced here: 36.6 us
  Pallas kernels  35.8 us (96%)
  local copies, waits for them, and re-layouts  0.8 us (2%)
    pallas_call x1, Pallas kernels, per_device(): pl.pallas_call(functools.partial(fused_kernel, devices, columns, wide, pi...  35.8 us
    unnamed x1, local copies, waits for them, and re-layouts  0.8 us

profile of v6, /device:TPU:27, one launch (start us, length us, event | category | flops | bytes accessed | tf_op | source)
XLA Modules:
  0.0 36.6 jit_solution(16154157547214181078)
XLA Ops:
  0.0 35.8 %fused_mixer.1 = bf16[128,2048]{1,0:T(8,128)(2,1)S(1)} custom-call(bf16[128,2048]{1,0:T(8,128)(2,1)} %bitcast.9, bf16[128,2048]{1,0:T(8,128)(2,1)} %bitcast.10, bf16[128,2048]{1,0:T(8,128)(2,1)} %bitcast.11, bf16[128,128]{1,0:T(8,128)(2,1)} %bitcast.12, bf16[128,128]{1,0:T(8,128)(2,1)} %bitcast.13, bf16[128,2048]{1,0:T(8,128)(2,1)} %dup_hbm.1, ...), custom_call_target="tpu_custom_call" | custom-call | tf_op jit(solution)/shard_map/fused_mixer/pallas_call | solution.py:602
  35.8 0.8 %copy.12 = bf16[1,128,2048]{2,1,0:T(8,128)(2,1)} copy(bf16[1,128,2048]{2,1,0:T(8,128)(2,1)S(1)} %bitcast.8) | data formatting | bytes 1048576
